TPU v7x, 32 devices: a whole 2x2x4 slice. The times are simulated.
32 devices in a mesh: ep: 16 (over z, x, core), tp: 2 (over y).
Axes of the slice: x: 2, y: 2, z: 4, core: 2. Of those that a mesh axis runs over, the one named last changes fastest.
Arguments:
- tokens: bfloat16 [256, 1024], P('ep'), may hold values from -6 to 6
- old_state: float32 [256, 4, 128, 128], P('ep', 'tp'), may hold values from -6 to 6
- query_weight: bfloat16 [1024, 512], P(None, 'tp'), may hold values from -0.1875 to 0.1875
- forget_weight: bfloat16 [1024, 512], P(None, 'tp'), may hold values from -0.1875 to 0.1875
- input_weight: bfloat16 [1024, 512], P(None, 'tp'), may hold values from -0.1875 to 0.1875
- lower_bound: float32 [512], P('tp'), may hold values from 0 to 0.9
- head_gain: float32 [4, 128], P('tp'), may hold values from 0.1 to 1.9
- out_weight: bfloat16 [512, 1024], P('tp'), may hold values from -0.25 to 0.25
- mix_gain: float32 [1024], replicated, may hold values from 0.1 to 1.9
- ffn_gain: float32 [1024], replicated, may hold values from 0.1 to 1.9
- group_weight: bfloat16 [1024, 4], replicated, may hold values from -0.1875 to 0.1875
- expert_weight: bfloat16 [1024, 16], replicated, may hold values from -0.1875 to 0.1875
- routes: int32 [256, 6], P('ep'), may hold values from 0 to 15, all different within a row; in each aligned block of 16 rows (0 to 15, 16 to 31, ...) at most 12 rows name the same one
- gate_weight: bfloat16 [16, 1024, 1024], P('ep', None, 'tp'), may hold values from -0.1875 to 0.1875
- up_weight: bfloat16 [16, 1024, 1024], P('ep', None, 'tp'), may hold values from -0.1875 to 0.1875
- down_weight: bfloat16 [16, 1024, 1024], P('ep', None, 'tp'), may hold values from -0.1875 to 0.1875
Outputs:
- layer_out: bfloat16 [256, 1024], P('ep', 'tp')
- new_state: float32 [256, 4, 128, 128], P('ep', 'tp')
Inputs may be any that keep to these rules, and one draw needn't show every extreme that they name: `routes`: each row names 6 different experts. In each aligned block of 16 rows (the rows of one device) no expert is named more than 12 times, a bound that some block reaches.
All inputs are finite; a program needn't handle non-finite values.
Results may differ from a plain program's by a relative error of at most 0.011.
Values may be sent and summed in bfloat16 or wider, within the bound.
A program may use at most 64 MiB of HBM per device.

v0:
```python
import jax
import jax.numpy as jnp
from jax import lax
from jax.sharding import PartitionSpec as P

epsilon = 1e-06


def scaled_rms(values, gain):
    return values * lax.rsqrt(jnp.mean(values * values, axis=-1, keepdims=True) + epsilon) * gain


def local(
    tokens,
    old_state,
    query_weight,
    forget_weight,
    input_weight,
    lower_bound,
    head_gain,
    out_weight,
    mix_gain,
    ffn_gain,
    group_weight,
    expert_weight,
    routes,
    gate_weight,
    up_weight,
    down_weight,
):
    seq_count, model_width = tokens.shape
    heads_local, head_size = (old_state.shape[1], old_state.shape[2])
    tp_size = lax.axis_size("tp")
    tp_rank = lax.axis_index("tp")
    part_width = model_width // tp_size
    resident = tokens.astype(jnp.float32)
    normed = scaled_rms(resident, mix_gain).astype(jnp.bfloat16)
    query_pre = jnp.dot(normed, query_weight, preferred_element_type=jnp.float32)
    forget_pre = jnp.dot(normed, forget_weight, preferred_element_type=jnp.float32)
    input_pre = jnp.dot(normed, input_weight, preferred_element_type=jnp.float32)
    query = jax.nn.silu(query_pre).reshape(seq_count, heads_local, head_size)
    forget = (lower_bound + (1.0 - lower_bound) * jax.nn.sigmoid(forget_pre)).reshape(
        seq_count, heads_local, head_size
    )
    value = input_pre.reshape(seq_count, heads_local, head_size)
    new_state = forget[..., None] * old_state + (1.0 - forget)[..., None] * value[:, :, None, :]
    readout = jnp.sum(new_state * query[..., None], axis=2)
    head_out = (
        scaled_rms(readout, head_gain)
        .astype(jnp.bfloat16)
        .reshape(seq_count, heads_local * head_size)
    )
    head_part = jnp.dot(head_out, out_weight, preferred_element_type=jnp.float32)
    mixed = lax.psum(head_part.astype(jnp.bfloat16), "tp")
    residual = (resident + mixed.astype(jnp.float32)).astype(jnp.bfloat16)
    ffn_in = scaled_rms(residual.astype(jnp.float32), ffn_gain).astype(jnp.bfloat16)
    experts = expert_weight.shape[1]
    groups = group_weight.shape[1]
    top_count = routes.shape[1]
    group_raw = jnp.exp(jnp.dot(ffn_in, group_weight, preferred_element_type=jnp.float32))
    group_prob = group_raw / jnp.sum(group_raw, axis=-1, keepdims=True)
    expert_raw = jnp.exp(
        jnp.dot(ffn_in, expert_weight, preferred_element_type=jnp.float32)
    ).reshape(seq_count, groups, experts // groups)
    expert_prob = (
        expert_raw / jnp.sum(expert_raw, axis=-1, keepdims=True) * group_prob[:, :, None]
    ).reshape(seq_count, experts)
    expert_ids = jnp.arange(experts, dtype=jnp.int32)
    chosen = routes[:, :, None] == expert_ids[None, None, :]
    weight = jnp.sum(jnp.where(chosen, expert_prob[:, None, :], 0.0), axis=-1)
    gate = weight / jnp.sum(weight, axis=-1, keepdims=True)
    capacity = min(seq_count, max(2, 2 * seq_count * top_count // experts))
    flat = routes.reshape(-1)
    hits = (flat[:, None] == expert_ids[None, :]).astype(jnp.int32)
    before = jnp.cumsum(hits, axis=0) - hits
    slots = jnp.sum(hits * before, axis=1)
    target = flat * capacity + slots
    slot_ids = jnp.arange(experts * capacity, dtype=jnp.int32)
    spread = jnp.sum(
        (slot_ids[:, None, None] == target.reshape(seq_count, top_count)[None, :, :]).astype(
            jnp.int32
        ),
        axis=2,
    ).astype(jnp.bfloat16)
    choose = (target[:, None] == slot_ids[None, :]).astype(jnp.bfloat16)
    outgoing = (
        jnp.dot(spread, ffn_in, preferred_element_type=jnp.float32)
        .astype(jnp.bfloat16)
        .reshape(experts, capacity, model_width)
    )
    arrived = lax.all_to_all(outgoing, "ep", split_axis=0, concat_axis=1, tiled=True)
    gate_hidden = jnp.einsum(
        "erd,edf->erf", arrived, gate_weight, preferred_element_type=jnp.float32
    )
    up_hidden = jnp.einsum("erd,edf->erf", arrived, up_weight, preferred_element_type=jnp.float32)
    hidden = (jax.nn.silu(gate_hidden) * up_hidden).astype(jnp.bfloat16)
    produced = jnp.einsum(
        "erf,efd->erd",
        lax.all_gather(hidden, "tp", axis=2, tiled=True),
        down_weight,
        preferred_element_type=jnp.float32,
    ).astype(jnp.bfloat16)
    returned = lax.all_to_all(produced, "ep", split_axis=1, concat_axis=0, tiled=True)
    picked = jnp.dot(
        choose, returned.reshape(experts * capacity, part_width), preferred_element_type=jnp.float32
    ).reshape(seq_count, top_count, part_width)
    mixture = jnp.sum(gate[:, :, None] * picked, axis=1)
    own_resid = lax.dynamic_slice_in_dim(residual, tp_rank * part_width, part_width, 1).astype(
        jnp.float32
    )
    layer_out = (own_resid + mixture).astype(jnp.bfloat16)
    return (layer_out, new_state)


def solution(mesh):
    in_specs = (
        P("ep", None),
        P("ep", "tp", None, None),
        P(None, "tp"),
        P(None, "tp"),
        P(None, "tp"),
        P("tp"),
        P("tp", None),
        P("tp", None),
        P(),
        P(),
        P(),
        P(),
        P("ep", None),
        P("ep", None, "tp"),
        P("ep", None, "tp"),
        P("ep", None, "tp"),
    )
    out_specs = (P("ep", "tp"), P("ep", "tp", None, None))
    return jax.shard_map(local, mesh=mesh, in_specs=in_specs, out_specs=out_specs, check_vma=False)
```

profile of v0, /device:TPU:0, one launch (start us, length us, event | category | flops | bytes accessed | tf_op | source)
XLA Modules:
  0.0 71.4 jit_solution(7429910828382578727)
XLA Ops:
  0.7 0.9 %copy.77 = s32[16,6]{1,0:T(8,128)S(1)} copy(s32[16,6]{0,1:T(8,128)} %param.28) | data formatting | bytes 768 | tf_op args[12]
  1.8 0.1 reduce_window_sum.11
  1.9 0.2 select_reduce_fusion.2
  2.2 0.7 multiply_add_fusion.1
  3.0 0.9 %fusion.20 = f32[16]{0:T(128)S(1)} fusion(bf16[16,1024]{1,0:T(8,128)(2,1)} %param.16), kind=kLoop, calls=%fused_computation.37 | loop fusion | flops 49136 | bytes 32832 | tf_op jit(solution)/shard_map/reduce_sum | solution.py:10
  3.9 1.3 %divide_multiply_fusion = f32[16,256]{1,0:T(8,128)S(1)} fusion(bf16[1024,256]{1,0:T(8,128)(2,1)} %param.18, bf16[16,1024]{1,0:T(8,128)(2,1)} %param.16, f32[1024]{0:T(1024)} %param.24, f32[16]{0:T(128)S(1)} %add_rsqrt_fusion.2), kind=kOutput, calls=%fused_computation.53 | convolution fusion | flops 8470528 | bytes 577600 | tf_op jit(solution)/shard_map/dot_general | solution.py:38
  5.3 1.3 %fusion.33 = f32[16,256]{1,0:T(8,128)S(1)} fusion(bf16[1024,256]{1,0:T(8,128)(2,1)} %param.20, bf16[16,1024]{1,0:T(8,128)(2,1)} %param.16, f32[1024]{0:T(1024)} %param.24, f32[16]{0:T(128)S(1)} %add_rsqrt_fusion.2), kind=kOutput, calls=%fused_computation.67 | convolution fusion | flops 8454144 | bytes 577600 | tf_op jit(solution)/shard_map/dot_general | solution.py:40
  6.6 0.7 broadcast_subtract_fusion.1
  7.3 1.3 %fusion.8 = f32[16,256]{1,0:T(8,128)S(1)} fusion(bf16[1024,256]{1,0:T(8,128)(2,1)} %param.19, f32[256]{0:T(256)S(1)} %broadcast_subtract_fusion.1, f32[256]{0:T(256)} %param.21, bf16[16,1024]{1,0:T(8,128)(2,1)} %param.16, f32[1024]{0:T(1024)} %param.24, f32[16]{0:T(128)S(1)} %add_rsqrt_fusion.2), kind=kOutput, calls=%fused_computation.16 | convolution fusion | flops 8474624 | bytes 579648 | tf_op jit(solution)/shard_map/dot_general | solution.py:39
  8.7 3.0 %multiply_reduce_fusion = (f32[16,2,128]{2,1,0:T(2,128)S(1)}, f32[16,2,128,128]{3,2,1,0:T(8,128)}) fusion(f32[16,2,128]{2,1,0:T(2,128)S(1)} %mul.173, f32[16,2,128]{2,1,0:T(2,128)S(1)} %mul.169, f32[16,2,128]{2,1,0:T(2,128)S(1)} %broadcast_subtract_fusion, f32[16,2,128,128]{3,2,1,0:T(8,128)S(1)} %copy-done.1, f32[16,2,128]{2,1,0:T(2,128)S(1)} %mul.165), kind=kLoop, calls=%fused_computation.1 | loop fusion | flops 2617344 | bytes 4276224 | tf_op jit(solution)/shard_map/reduce_sum | solution.py:47
  12.0 1.2 %convolution_convert_fusion.2 = bf16[16,1024]{1,0:T(8,128)(2,1)S(1)} fusion(bf16[256,1024]{1,0:T(8,128)(2,1)} %param.23, f32[2,8,2,128]{3,2,1,0:T(2,128)S(1)} %bitcast.43, f32[256]{0:T(256)S(1)} %bitcast.47), kind=kOutput, calls=%fused_computation.10 | convolution fusion | flops 8413184 | bytes 574464 | tf_op jit(solution)/shard_map/dot_general | solution.py:53
  13.2 10.0 %psum.7 = bf16[16,1024]{1,0:T(8,128)(2,1)S(1)} all-reduce(bf16[16,1024]{1,0:T(8,128)(2,1)S(1)} %convolution_convert_fusion.2), channel_id=1, replica_groups=mesh['ep'=16,'tp'=2] {'tp'}, use_global_device_ids=true, to_apply=%region_3.4 | all-reduce | flops 16384 | bytes 65536 | tf_op jit(solution)/shard_map/psum | solution.py:54
  23.3 0.3 convolution_convert_fusion
  23.6 0.9 %reshape.168 = bf16[16,12,1024]{2,1,0:T(8,128)(2,1)} reshape(bf16[192,1024]{1,0:T(8,128)(2,1)S(1)} %convolution_convert_fusion) | data formatting | bytes 786432 | tf_op jit(solution)/shard_map/reshape | solution.py:89
  24.5 5.9 %all-to-all-start = ((bf16[16,12,1024]{2,1,0:T(8,128)(2,1)}), bf16[16,12,1024]{2,1,0:T(8,128)(2,1)S(1)}, u32[]{:S(2)}, u32[]{:S(2)}) async-start(bf16[16,12,1024]{2,1,0:T(8,128)(2,1)} %reshape.168), calls=%async_computation | async-start | bytes 1048576 | tf_op jit(solution)/shard_map/all_to_all | solution.py:91
  30.5 0.2 fusion.42
  30.8 0.2 convolution_exponential_fusion
  31.1 13.6 %all-to-all-done = bf16[16,12,1024]{2,1,0:T(8,128)(2,1)S(1)} async-done(((bf16[16,12,1024]{2,1,0:T(8,128)(2,1)}), bf16[16,12,1024]{2,1,0:T(8,128)(2,1)S(1)}, u32[]{:S(2)}, u32[]{:S(2)}) %all-to-all-start) | async-done | bytes 393248 | tf_op jit(solution)/shard_map/all_to_all | solution.py:91
  44.8 0.4 fusion.11
  45.2 0.4 fusion.1
  45.6 7.6 %all-gather = bf16[192,1024]{1,0:T(8,128)(2,1)S(1)} all-gather(bf16[192,512]{1,0:T(8,128)(2,1)S(1)} %fusion.1), channel_id=2, replica_groups=mesh['ep'=16,'tp'=2] {'tp'}, dimensions={1}, use_global_device_ids=true | all-gather | bytes 589824 | tf_op jit(solution)/shard_map/all_gather | solution.py:99
  53.2 0.4 fusion.2
  53.6 0.3 copy.92
  53.9 0.5 broadcast.119
  54.4 1.8 %reduce.1 = bf16[192,512]{1,0:T(8,128)(2,1)S(1)} reduce(bf16[192,1,512]{2,1,0:T(2,128)(2,1)S(1)} %bitcast.41, bf16[]{:T(256)} %broadcast.119), dimensions={1}, to_apply=%bitcast.40.reduce_sub_computation | reduce | bytes 393218
  56.3 0.8 %reshape.179 = bf16[16,2,3072]{2,1,0:T(2,128)(2,1)} reshape(bf16[192,512]{1,0:T(8,128)(2,1)S(1)} %reduce.1) | data formatting | bytes 393216
  57.0 4.4 %all-to-all-start.1 = ((bf16[16,2,3072]{2,1,0:T(2,128)(2,1)}), bf16[16,2,3072]{2,1,0:T(2,128)(2,1)S(1)}, u32[]{:S(2)}, u32[]{:S(2)}) async-start(bf16[16,2,3072]{2,1,0:T(2,128)(2,1)} %reshape.179), calls=%async_computation.1 | async-start | bytes 393216 | tf_op jit(solution)/shard_map/all_to_all | solution.py:103
  61.5 0.2 select_reduce_fusion
  61.7 8.7 %all-to-all-done.1 = bf16[16,2,3072]{2,1,0:T(2,128)(2,1)S(1)} async-done(((bf16[16,2,3072]{2,1,0:T(2,128)(2,1)}), bf16[16,2,3072]{2,1,0:T(2,128)(2,1)S(1)}, u32[]{:S(2)}, u32[]{:S(2)}) %all-to-all-start.1) | async-done | bytes 196640 | tf_op jit(solution)/shard_map/all_to_all | solution.py:103
  70.4 0.1 reshape.180
  70.5 0.2 fusion.3
  70.8 0.6 add_convert_fusion
  (45 shorter events, 1.3 us)
Async XLA Ops:
  0.6 44.2 %copy-start = (bf16[1,1024,512]{2,1,0:T(8,128)(2,1)S(1)}, bf16[1,1024,512]{2,1,0:T(8,128)(2,1)}, u32[]{:S(2)}) copy-start(bf16[1,1024,512]{2,1,0:T(8,128)(2,1)} %param.29) | copy-start | bytes 3145732
  0.6 8.0 %copy-start.1 = (f32[16,2,128,128]{3,2,1,0:T(8,128)S(1)}, f32[16,2,128,128]{3,2,1,0:T(8,128)}, u32[]{:S(2)}) copy-start(f32[16,2,128,128]{3,2,1,0:T(8,128)} %param.17) | copy-start | bytes 6291460
  8.6 3.4 %copy-start.6 = (f32[2,128]{1,0:T(2,128)S(1)}, f32[2,128]{1,0:T(2,128)}, u32[]{:S(2)}) copy-start(f32[2,128]{1,0:T(2,128)} %param.22) | copy-start | bytes 3076
  8.6 14.5 %copy-start.3 = (bf16[16,1024]{1,0:T(8,128)(2,1)S(1)}, bf16[16,1024]{1,0:T(8,128)(2,1)}, u32[]{:S(2)}) copy-start(bf16[16,1024]{1,0:T(8,128)(2,1)} %param.16) | copy-start | bytes 98308
  8.7 14.7 %copy-start.5 = (f32[1024]{0:T(1024)S(1)}, f32[1024]{0:T(1024)}, u32[]{:S(2)}) copy-start(f32[1024]{0:T(1024)} %param.25) | copy-start | bytes 12292
  11.7 18.8 %copy-start.9 = (bf16[1024,4]{0,1:T(4,128)(2,1)S(1)}, bf16[1024,4]{0,1:T(4,128)(2,1)}, u32[]{:S(2)}) copy-start(bf16[1024,4]{0,1:T(4,128)(2,1)} %param.26) | copy-start | bytes 24580
  11.7 19.1 %copy-start.8 = (bf16[1024,16]{0,1:T(8,128)(2,1)S(1)}, bf16[1024,16]{0,1:T(8,128)(2,1)}, u32[]{:S(2)}) copy-start(bf16[1024,16]{0,1:T(8,128)(2,1)} %param.27) | copy-start | bytes 98308
  24.5 20.7 %copy-start.7 = (bf16[1,1024,512]{2,1,0:T(8,128)(2,1)S(1)}, bf16[1,1024,512]{2,1,0:T(8,128)(2,1)}, u32[]{:S(2)}) copy-start(bf16[1,1024,512]{2,1,0:T(8,128)(2,1)} %param.30) | copy-start | bytes 3145732
  24.5 20.2 %all-to-all-start = ((bf16[16,12,1024]{2,1,0:T(8,128)(2,1)}), bf16[16,12,1024]{2,1,0:T(8,128)(2,1)S(1)}, u32[]{:S(2)}, u32[]{:S(2)}) async-start(bf16[16,12,1024]{2,1,0:T(8,128)(2,1)} %reshape.168), calls=%async_computation | async-start | bytes 1048576 | tf_op jit(solution)/shard_map/all_to_all | solution.py:91
  45.2 8.0 %copy-start.2 = (bf16[1,1024,512]{2,1,0:T(8,128)(2,1)S(1)}, bf16[1,1024,512]{2,1,0:T(8,128)(2,1)}, u32[]{:S(2)}) copy-start(bf16[1,1024,512]{2,1,0:T(8,128)(2,1)} %param.31) | copy-start | bytes 3145732
  45.6 15.8 %copy-start.4 = (s32[16,6]{0,1:T(8,128)S(1)}, s32[16,6]{0,1:T(8,128)}, u32[]{:S(2)}) copy-start(s32[16,6]{0,1:T(8,128)} %param.28) | copy-start | bytes 1156
  57.0 13.4 %all-to-all-start.1 = ((bf16[16,2,3072]{2,1,0:T(2,128)(2,1)}), bf16[16,2,3072]{2,1,0:T(2,128)(2,1)S(1)}, u32[]{:S(2)}, u32[]{:S(2)}) async-start(bf16[16,2,3072]{2,1,0:T(2,128)(2,1)} %reshape.179), calls=%async_computation.1 | async-start | bytes 393216 | tf_op jit(solution)/shard_map/all_to_all | solution.py:103
where the time goes:
time: 71.9 us; the launch traced here: 71.4 us
  waiting for transfers between devices  22.3 us (31%)
  blocking collectives  17.6 us (24%)
  starting transfers between devices  10.3 us (14%)
  other arithmetic  8.77 us (12%)
  matrix products  7.21 us (10%)
  local copies, waits for them, and re-layouts  4.28 us (6%)
  between operations  0.95 us (1%)
    all_to_all x1, waiting for transfers between devices, local(): lax.all_to_all(outgoing, 'ep', split_axis=0, concat_axis=1, tiled=True)  13.6 us
    psum x1, blocking collectives, local(): mixed = lax.psum(head_part.astype(jnp.bfloat16), 'tp')  9.95 us
    all_to_all x1, waiting for transfers between devices, local(): lax.all_to_all(produced, 'ep', split_axis=1, concat_axis=0, tiled=True)  8.72 us
    all_gather x1, blocking collectives, local(): lax.all_gather(hidden, 'tp', axis=2, tiled=True)  7.6 us
    all_to_all x1, starting transfers between devices, local(): lax.all_to_all(outgoing, 'ep', split_axis=0, concat_axis=1, tiled=True)  5.92 us
    all_to_all x1, starting transfers between devices, local(): lax.all_to_all(produced, 'ep', split_axis=1, concat_axis=0, tiled=True)  4.41 us
    reduce_sum x1, other arithmetic, local(): readout = jnp.sum(new_state * query[..., None], axis=2)  3.02 us
    unnamed x24, local copies, waits for them, and re-layouts  2.4 us
  transfers between devices with their start and end apart: 2, of which 2 were waited for; matrix products, arithmetic and copies ran while one was open for 1% of the time, Pallas kernels for 0%

commit v1 on v0

--- a/solution.py
+++ b/solution.py
@@ -2,6 +2,7 @@
 import jax.numpy as jnp
 from jax import lax
 from jax.sharding import PartitionSpec as P
+from jax.lax import all_gather
 
 epsilon = 1e-06
 
@@ -51,7 +52,12 @@
         .reshape(seq_count, heads_local * head_size)
     )
     head_part = jnp.dot(head_out, out_weight, preferred_element_type=jnp.float32)
-    mixed = lax.psum(head_part.astype(jnp.bfloat16), "tp")
+
+    def trace_steps_all_all(z, dev_axis):
+        vec_out = all_gather(z, axis_name=dev_axis)
+        return jnp.sum(vec_out, axis=0)
+
+    mixed = trace_steps_all_all(head_part.astype(jnp.bfloat16), "tp")
     residual = (resident + mixed.astype(jnp.float32)).astype(jnp.bfloat16)
     ffn_in = scaled_rms(residual.astype(jnp.float32), ffn_gain).astype(jnp.bfloat16)
     experts = expert_weight.shape[1]

time: 71.9 us -> 68.2 us (0.949)
  blocking collectives: 17.6 us -> 13.2 us
    psum x1 -> x0, blocking collectives: 9.95 us -> none  [local(): mixed = lax.psum(head_part.astype(jnp.bfloat16), 'tp')]
    all_gather x0 -> x1, blocking collectives: none -> 5.53 us  [trace_steps_all_all(): vec_out = all_gather(z, axis_name=dev_axis)]
where the time goes in v1:
time: 68.2 us; the launch traced here: 67.6 us
  waiting for transfers between devices  22.3 us (33%)
  blocking collectives  13.2 us (19%)
  starting transfers between devices  11 us (16%)
  other arithmetic  8.78 us (13%)
  matrix products  7.19 us (11%)
  local copies, waits for them, and re-layouts  4.28 us (6%)
  between operations  0.95 us (1%)
    all_to_all x1, waiting for transfers between devices, local(): lax.all_to_all(outgoing, 'ep', split_axis=0, concat_axis=1, tiled=True)  13.6 us
    all_to_all x1, waiting for transfers between devices, local(): lax.all_to_all(produced, 'ep', split_axis=1, concat_axis=0, tiled=True)  8.72 us
    all_gather x1, blocking collectives, local(): lax.all_gather(hidden, 'tp', axis=2, tiled=True)  7.62 us
    all_to_all x1, starting transfers between devices, local(): lax.all_to_all(outgoing, 'ep', split_axis=0, concat_axis=1, tiled=True)  6.57 us
    all_gather x1, blocking collectives, trace_steps_all_all(): vec_out = all_gather(z, axis_name=dev_axis)  5.53 us
    all_to_all x1, starting transfers between devices, local(): lax.all_to_all(produced, 'ep', split_axis=1, concat_axis=0, tiled=True)  4.41 us
    reduce_sum x1, other arithmetic, local(): readout = jnp.sum(new_state * query[..., None], axis=2)  3.02 us
    unnamed x24, local copies, waits for them, and re-layouts  2.4 us
  transfers between devices with their start and end apart: 2, of which 2 were waited for; matrix products, arithmetic and copies ran while one was open for 1% of the time, Pallas kernels for 0%

profile of v1, /device:TPU:0, one launch (start us, length us, event | category | flops | bytes accessed | tf_op | source)
XLA Modules:
  0.0 67.6 jit_solution(4205302458017341384)
XLA Ops:
  0.7 0.9 %copy.77 = s32[16,6]{1,0:T(8,128)S(1)} copy(s32[16,6]{0,1:T(8,128)} %param.28) | data formatting | bytes 768 | tf_op args[12]
  1.8 0.1 reduce_window_sum.11
  1.9 0.2 select_reduce_fusion.2
  2.2 0.7 %multiply_add_fusion.1 = s32[16,6]{0,1:T(8,128)S(1)} fusion(s32[16,6]{0,1:T(8,128)S(1)} %copy.78, s32[16,6]{0,1:T(8,128)} %param.28), kind=kLoop, calls=%fused_computation.59 | loop fusion | flops 192 | bytes 1152 | tf_op jit(solution)/shard_map/add | solution.py:83
  3.0 0.9 %fusion.20 = f32[16]{0:T(128)S(1)} fusion(bf16[16,1024]{1,0:T(8,128)(2,1)} %param.16), kind=kLoop, calls=%fused_computation.37 | loop fusion | flops 49136 | bytes 32832 | tf_op jit(solution)/shard_map/reduce_sum | solution.py:11
  3.9 1.3 %divide_multiply_fusion = f32[16,256]{1,0:T(8,128)S(1)} fusion(bf16[1024,256]{1,0:T(8,128)(2,1)} %param.18, bf16[16,1024]{1,0:T(8,128)(2,1)} %param.16, f32[1024]{0:T(1024)} %param.24, f32[16]{0:T(128)S(1)} %add_rsqrt_fusion.2), kind=kOutput, calls=%fused_computation.53 | convolution fusion | flops 8470528 | bytes 577600 | tf_op jit(solution)/shard_map/dot_general | solution.py:39
  5.3 1.3 %fusion.33 = f32[16,256]{1,0:T(8,128)S(1)} fusion(bf16[1024,256]{1,0:T(8,128)(2,1)} %param.20, bf16[16,1024]{1,0:T(8,128)(2,1)} %param.16, f32[1024]{0:T(1024)} %param.24, f32[16]{0:T(128)S(1)} %add_rsqrt_fusion.2), kind=kOutput, calls=%fused_computation.67 | convolution fusion | flops 8454144 | bytes 577600 | tf_op jit(solution)/shard_map/dot_general | solution.py:41
  6.6 0.7 %broadcast_subtract_fusion.1 = f32[256]{0:T(256)S(1)} fusion(f32[256]{0:T(256)} %param.21), kind=kLoop, calls=%fused_computation.65 | loop fusion | flops 256 | bytes 2048 | tf_op jit(solution)/shard_map/sub | solution.py:43
  7.3 1.3 %fusion.8 = f32[16,256]{1,0:T(8,128)S(1)} fusion(bf16[1024,256]{1,0:T(8,128)(2,1)} %param.19, f32[256]{0:T(256)S(1)} %broadcast_subtract_fusion.1, f32[256]{0:T(256)} %param.21, bf16[16,1024]{1,0:T(8,128)(2,1)} %param.16, f32[1024]{0:T(1024)} %param.24, f32[16]{0:T(128)S(1)} %add_rsqrt_fusion.2), kind=kOutput, calls=%fused_computation.16 | convolution fusion | flops 8474624 | bytes 579648 | tf_op jit(solution)/shard_map/dot_general | solution.py:40
  8.7 3.0 %multiply_reduce_fusion = (f32[16,2,128]{2,1,0:T(2,128)S(1)}, f32[16,2,128,128]{3,2,1,0:T(8,128)}) fusion(f32[16,2,128]{2,1,0:T(2,128)S(1)} %mul.173, f32[16,2,128]{2,1,0:T(2,128)S(1)} %mul.169, f32[16,2,128]{2,1,0:T(2,128)S(1)} %broadcast_subtract_fusion, f32[16,2,128,128]{3,2,1,0:T(8,128)S(1)} %copy-done.1, f32[16,2,128]{2,1,0:T(2,128)S(1)} %mul.165), kind=kLoop, calls=%fused_computation.1 | loop fusion | flops 2617344 | bytes 4276224 | tf_op jit(solution)/shard_map/reduce_sum | solution.py:48
  12.0 1.2 %convolution_convert_fusion.2 = bf16[16,1024]{1,0:T(8,128)(2,1)S(1)} fusion(bf16[256,1024]{1,0:T(8,128)(2,1)} %param.23, f32[2,8,2,128]{3,2,1,0:T(2,128)S(1)} %bitcast.45, f32[256]{0:T(256)S(1)} %bitcast.49), kind=kOutput, calls=%fused_computation.10 | convolution fusion | flops 8413184 | bytes 574464 | tf_op jit(solution)/shard_map/dot_general | solution.py:54
  13.2 5.5 %all-gather = bf16[32,1024]{1,0:T(8,128)(2,1)S(1)} all-gather(bf16[16,1024]{1,0:T(8,128)(2,1)S(1)} %convolution_convert_fusion.2), channel_id=2, replica_groups=mesh['ep'=16,'tp'=2] {'tp'}, dimensions={0}, use_global_device_ids=true | all-gather | bytes 98304 | tf_op jit(solution)/shard_map/all_gather | solution.py:57
  18.9 0.3 convolution_convert_fusion
  19.2 0.9 %reshape.168 = bf16[16,12,1024]{2,1,0:T(8,128)(2,1)} reshape(bf16[192,1024]{1,0:T(8,128)(2,1)S(1)} %convolution_convert_fusion) | data formatting | bytes 786432 | tf_op jit(solution)/shard_map/reshape | solution.py:95
  20.1 6.6 %all-to-all-start = ((bf16[16,12,1024]{2,1,0:T(8,128)(2,1)}), bf16[16,12,1024]{2,1,0:T(8,128)(2,1)S(1)}, u32[]{:S(2)}, u32[]{:S(2)}) async-start(bf16[16,12,1024]{2,1,0:T(8,128)(2,1)} %reshape.168), calls=%async_computation | async-start | bytes 1048576 | tf_op jit(solution)/shard_map/all_to_all | solution.py:97
  26.7 0.2 fusion.42
  27.0 0.2 convolution_exponential_fusion
  27.4 13.6 %all-to-all-done = bf16[16,12,1024]{2,1,0:T(8,128)(2,1)S(1)} async-done(((bf16[16,12,1024]{2,1,0:T(8,128)(2,1)}), bf16[16,12,1024]{2,1,0:T(8,128)(2,1)S(1)}, u32[]{:S(2)}, u32[]{:S(2)}) %all-to-all-start) | async-done | bytes 393248 | tf_op jit(solution)/shard_map/all_to_all | solution.py:97
  41.1 0.4 fusion.11
  41.5 0.4 fusion.1
  41.8 7.6 %all-gather.1 = bf16[192,1024]{1,0:T(8,128)(2,1)S(1)} all-gather(bf16[192,512]{1,0:T(8,128)(2,1)S(1)} %fusion.1), channel_id=3, replica_groups=mesh['ep'=16,'tp'=2] {'tp'}, dimensions={1}, use_global_device_ids=true | all-gather | bytes 589824 | tf_op jit(solution)/shard_map/all_gather | solution.py:105
  49.5 0.4 fusion.2
  49.9 0.3 copy.92
  50.2 0.5 broadcast.119
  50.7 1.8 %reduce.2 = bf16[192,512]{1,0:T(8,128)(2,1)S(1)} reduce(bf16[192,1,512]{2,1,0:T(2,128)(2,1)S(1)} %bitcast.42, bf16[]{:T(256)} %broadcast.119), dimensions={1}, to_apply=%bitcast.41.reduce_sub_computation | reduce | bytes 393218
  52.5 0.8 %reshape.180 = bf16[16,2,3072]{2,1,0:T(2,128)(2,1)} reshape(bf16[192,512]{1,0:T(8,128)(2,1)S(1)} %reduce.2) | data formatting | bytes 393216
  53.3 4.4 %all-to-all-start.1 = ((bf16[16,2,3072]{2,1,0:T(2,128)(2,1)}), bf16[16,2,3072]{2,1,0:T(2,128)(2,1)S(1)}, u32[]{:S(2)}, u32[]{:S(2)}) async-start(bf16[16,2,3072]{2,1,0:T(2,128)(2,1)} %reshape.180), calls=%async_computation.1 | async-start | bytes 393216 | tf_op jit(solution)/shard_map/all_to_all | solution.py:109
  57.7 0.2 select_reduce_fusion
  57.9 8.7 %all-to-all-done.1 = bf16[16,2,3072]{2,1,0:T(2,128)(2,1)S(1)} async-done(((bf16[16,2,3072]{2,1,0:T(2,128)(2,1)}), bf16[16,2,3072]{2,1,0:T(2,128)(2,1)S(1)}, u32[]{:S(2)}, u32[]{:S(2)}) %all-to-all-start.1) | async-done | bytes 196640 | tf_op jit(solution)/shard_map/all_to_all | solution.py:109
  66.6 0.1 reshape.181
  66.8 0.2 fusion.3
  67.0 0.6 add_convert_fusion
  (46 shorter events, 1.3 us)
Async XLA Ops:
  0.6 40.4 %copy-start = (bf16[1,1024,512]{2,1,0:T(8,128)(2,1)S(1)}, bf16[1,1024,512]{2,1,0:T(8,128)(2,1)}, u32[]{:S(2)}) copy-start(bf16[1,1024,512]{2,1,0:T(8,128)(2,1)} %param.29) | copy-start | bytes 3145732
  0.6 8.0 %copy-start.1 = (f32[16,2,128,128]{3,2,1,0:T(8,128)S(1)}, f32[16,2,128,128]{3,2,1,0:T(8,128)}, u32[]{:S(2)}) copy-start(f32[16,2,128,128]{3,2,1,0:T(8,128)} %param.17) | copy-start | bytes 6291460
  8.6 3.4 %copy-start.6 = (f32[2,128]{1,0:T(2,128)S(1)}, f32[2,128]{1,0:T(2,128)}, u32[]{:S(2)}) copy-start(f32[2,128]{1,0:T(2,128)} %param.22) | copy-start | bytes 3076
  8.6 10.1 %copy-start.3 = (bf16[16,1024]{1,0:T(8,128)(2,1)S(1)}, bf16[16,1024]{1,0:T(8,128)(2,1)}, u32[]{:S(2)}) copy-start(bf16[16,1024]{1,0:T(8,128)(2,1)} %param.16) | copy-start | bytes 98308
  8.7 10.3 %copy-start.5 = (f32[1024]{0:T(1024)S(1)}, f32[1024]{0:T(1024)}, u32[]{:S(2)}) copy-start(f32[1024]{0:T(1024)} %param.25) | copy-start | bytes 12292
  11.7 15.0 %copy-start.9 = (bf16[1024,4]{0,1:T(4,128)(2,1)S(1)}, bf16[1024,4]{0,1:T(4,128)(2,1)}, u32[]{:S(2)}) copy-start(bf16[1024,4]{0,1:T(4,128)(2,1)} %param.26) | copy-start | bytes 24580
  11.7 15.3 %copy-start.8 = (bf16[1024,16]{0,1:T(8,128)(2,1)S(1)}, bf16[1024,16]{0,1:T(8,128)(2,1)}, u32[]{:S(2)}) copy-start(bf16[1024,16]{0,1:T(8,128)(2,1)} %param.27) | copy-start | bytes 98308
  20.1 21.3 %copy-start.7 = (bf16[1,1024,512]{2,1,0:T(8,128)(2,1)S(1)}, bf16[1,1024,512]{2,1,0:T(8,128)(2,1)}, u32[]{:S(2)}) copy-start(bf16[1,1024,512]{2,1,0:T(8,128)(2,1)} %param.30) | copy-start | bytes 3145732
  20.1 20.8 %all-to-all-start = ((bf16[16,12,1024]{2,1,0:T(8,128)(2,1)}), bf16[16,12,1024]{2,1,0:T(8,128)(2,1)S(1)}, u32[]{:S(2)}, u32[]{:S(2)}) async-start(bf16[16,12,1024]{2,1,0:T(8,128)(2,1)} %reshape.168), calls=%async_computation | async-start | bytes 1048576 | tf_op jit(solution)/shard_map/all_to_all | solution.py:97
  41.4 8.0 %copy-start.2 = (bf16[1,1024,512]{2,1,0:T(8,128)(2,1)S(1)}, bf16[1,1024,512]{2,1,0:T(8,128)(2,1)}, u32[]{:S(2)}) copy-start(bf16[1,1024,512]{2,1,0:T(8,128)(2,1)} %param.31) | copy-start | bytes 3145732
  41.8 15.9 %copy-start.4 = (s32[16,6]{0,1:T(8,128)S(1)}, s32[16,6]{0,1:T(8,128)}, u32[]{:S(2)}) copy-start(s32[16,6]{0,1:T(8,128)} %param.28) | copy-start | bytes 1156
  53.3 13.4 %all-to-all-start.1 = ((bf16[16,2,3072]{2,1,0:T(2,128)(2,1)}), bf16[16,2,3072]{2,1,0:T(2,128)(2,1)S(1)}, u32[]{:S(2)}, u32[]{:S(2)}) async-start(bf16[16,2,3072]{2,1,0:T(2,128)(2,1)} %reshape.180), calls=%async_computation.1 | async-start | bytes 393216 | tf_op jit(solution)/shard_map/all_to_all | solution.py:109
